TPU v7x, 32 devices: a whole 2x2x4 slice. The times are simulated.
32 devices in a mesh: fs: 8 (over z, y), tp: 4 (over x, core).
Axes of the slice: x: 2, y: 2, z: 4, core: 2. Of those that a mesh axis runs over, the one named last changes fastest.
Arguments:
- later_input: bfloat16 [4096, 2048], P(('fs', 'tp')), may hold values from -6 to 6
- earlier_input: bfloat16 [4096, 2048], P('fs'), may hold values from -6 to 6
- earlier_hidden: bfloat16 [4096, 4096], P('fs', 'tp'), may hold values from -6 to 6
- cotangent: bfloat16 [4096, 2048], P('fs'), may hold values from -6 to 6
- up_weight: bfloat16 [2048, 4096], P('fs', 'tp'), may hold values from -0.125 to 0.125
- down_weight: bfloat16 [4096, 2048], P(('tp', 'fs')), may hold values from -0.09375 to 0.09375
- up_sum: float32 [2048, 4096], P('fs', 'tp'), may hold values from -4 to 4
- down_sum: float32 [4096, 2048], P(('tp', 'fs')), may hold values from -4 to 4
Outputs:
- later_output: bfloat16 [4096, 2048], P(('fs', 'tp'))
- later_hidden: bfloat16 [4096, 4096], P('fs', 'tp')
- earlier_grad: bfloat16 [4096, 2048], P(('fs', 'tp'))
- up_sum_next: float32 [2048, 4096], P('fs', 'tp')
- down_sum_next: float32 [4096, 2048], P(('tp', 'fs'))
All inputs are finite; a program needn't handle non-finite values.
Results may differ from a plain program's by a relative error of at most 0.0095.
Values may be sent and summed in bfloat16 or wider, within the bound.
A program may use at most 128 MiB of HBM per device.

v0:
```python
import jax
import jax.numpy as jnp
from jax import lax
from jax.sharding import PartitionSpec as P


def contract_last(left_rows, right_rows):
    return lax.dot_general(
        left_rows, right_rows, (((1,), (1,)), ((), ())), preferred_element_type=jnp.float32
    )


def contract_first(left_rows, right_rows):
    return lax.dot_general(
        left_rows, right_rows, (((0,), (0,)), ((), ())), preferred_element_type=jnp.float32
    )


def shards(
    later_input, earlier_input, earlier_hidden, cotangent, up_weight, down_weight, up_sum, down_sum
):
    gathered = lax.all_gather(later_input, "tp", axis=0, tiled=True)
    groups = lax.axis_size("fs")
    grad_scale = float(earlier_input.shape[0] * groups) ** (-0.5)
    lifted = jnp.maximum(earlier_hidden.astype(jnp.float32), 0.0)
    activation = (lifted * lifted).astype(jnp.bfloat16)
    up_front, down_front = (
        lax.all_gather(up_weight, "fs", axis=0, tiled=True),
        lax.all_gather(down_weight, "fs", axis=0, tiled=True),
    )
    later_hidden = jnp.dot(gathered, up_front, preferred_element_type=jnp.float32).astype(
        jnp.bfloat16
    )
    lifted_later = jnp.maximum(later_hidden.astype(jnp.float32), 0.0)
    act_later = (lifted_later * lifted_later).astype(jnp.bfloat16)
    rows_here = act_later
    later_output = lax.psum_scatter(
        jnp.dot(rows_here, down_front, preferred_element_type=jnp.float32).astype(jnp.bfloat16),
        "tp",
        scatter_dimension=0,
        tiled=True,
    )
    up_back, down_back = (up_front, down_front)
    act_slope = contract_last(cotangent, down_back)
    pre_grad = (2.0 * act_slope * lifted).astype(jnp.bfloat16)
    rows_here = pre_grad
    earlier_grad = lax.psum_scatter(
        contract_last(rows_here, up_back).astype(jnp.bfloat16),
        "tp",
        scatter_dimension=0,
        tiled=True,
    )
    columns = earlier_input
    up_total = lax.psum_scatter(
        contract_first(columns, pre_grad), "fs", scatter_dimension=0, tiled=True
    )
    earlier_grad, up_total = (earlier_grad, up_total)
    columns = activation
    down_total = lax.psum_scatter(
        contract_first(columns, cotangent), "fs", scatter_dimension=0, tiled=True
    )
    return (
        later_output,
        later_hidden,
        earlier_grad,
        up_sum + grad_scale * up_total,
        down_sum + grad_scale * down_total,
    )


def solution(mesh):
    in_specs = (
        P(("fs", "tp"), None),
        P("fs", None),
        P("fs", "tp"),
        P("fs", None),
        P("fs", "tp"),
        P(("tp", "fs"), None),
        P("fs", "tp"),
        P(("tp", "fs"), None),
    )
    out_specs = (
        P(("fs", "tp"), None),
        P("fs", "tp"),
        P(("fs", "tp"), None),
        P("fs", "tp"),
        P(("tp", "fs"), None),
    )
    return jax.shard_map(shards, mesh=mesh, in_specs=in_specs, out_specs=out_specs, check_vma=False)
```

profile of v0, /device:TPU:0, one launch (start us, length us, event | category | flops | bytes accessed | tf_op | source)
XLA Modules:
  0.0 557.7 jit_solution(5843369301261905202)
XLA Ops:
  7.2 0.7 all-gather.8.cloned.1.call-update
  8.0 0.7 all-gather.6.cloned.1.call-update
  8.7 0.7 all-gather.4.cloned.1.call-update
  9.5 6.9 %fusion = f32[1024,2048]{1,0:T(8,128)} fusion(bf16[512,2048]{1,0:T(8,128)(2,1)S(1)} %copy-done, bf16[512,1024]{1,0:T(8,128)(2,1)} %param.10), kind=kOutput, calls=%fused_computation.8 | convolution fusion | flops 2149580800 | bytes 11534336 | tf_op jit(solution)/shard_map/dot_general | solution.py:14
  16.3 0.0 reduce-scatter.9.cloned.1.call-start
  16.4 69.3 %all-gather.8.cloned.1.call-done = bf16[1024,2048]{1,0:T(8,128)(2,1)} async-done(((bf16[128,2048]{1,0:T(8,128)(2,1)}), bf16[1024,2048]{1,0:T(8,128)(2,1)}) %all-gather.8.cloned.1.call-update) | async-done | bytes 4194320 | tf_op jit(solution)/shard_map/all_gather | solution.py:29
  85.7 4.7 multiply_convert_fusion.1
  90.4 1.0 copy-done.5
  91.4 5.6 %convolution_bitcast_fusion = f32[2048,1024]{0,1:T(8,128)} fusion(bf16[512,1024]{1,0:T(8,128)(2,1)S(1)} %multiply_convert_fusion.1, bf16[512,2048]{1,0:T(8,128)(2,1)S(1)} %copy-done.2), kind=kOutput, calls=%fused_computation | convolution fusion | flops 2147483648 | bytes 11534336 | tf_op jit(solution)/shard_map/dot_general | solution.py:14
  97.1 62.1 %all-gather.6.cloned.1.call-done = bf16[2048,1024]{1,0:T(8,128)(2,1)} async-done(((bf16[256,1024]{1,0:T(8,128)(2,1)}), bf16[2048,1024]{1,0:T(8,128)(2,1)}) %all-gather.6.cloned.1.call-update) | async-done | bytes 4194320 | tf_op jit(solution)/shard_map/all_gather | solution.py:28
  159.1 5.9 %convolution_convert_fusion = bf16[512,2048]{1,0:T(8,128)(2,1)} fusion(bf16[512,1024]{1,0:T(8,128)(2,1)S(1)} %copy-done.6, bf16[2048,1024]{1,0:T(8,128)(2,1)} %all-gather.6.cloned.1.call-done), kind=kOutput, calls=%fused_computation.1 | convolution fusion | flops 2148532224 | bytes 7340032 | tf_op jit(solution)/shard_map/dot_general | solution.py:8
  165.1 0.2 reduce-scatter.5.cloned.1.call-start
  165.3 16.5 %all-gather.4.cloned.1.call-done = bf16[512,2048]{1,0:T(8,128)(2,1)} async-done(((bf16[128,2048]{1,0:T(8,128)(2,1)}), bf16[512,2048]{1,0:T(8,128)(2,1)}) %all-gather.4.cloned.1.call-update) | async-done | bytes 2097168 | tf_op jit(solution)/shard_map/all_gather | solution.py:22
  181.8 5.3 convolution_convert_fusion.2
  187.2 1.0 copy-done.4
  188.1 3.7 convolution_convert_fusion.1
  191.8 1.9 copy.13
  193.7 139.1 %reduce-scatter.11.cloned.1.call-done = f32[128,2048]{1,0:T(8,128)} async-done(((f32[1024,2048]{1,0:T(8,128)}), f32[128,2048]{1,0:T(8,128)}) %reduce-scatter.11.cloned.1.call-update) | async-done | bytes 1048592 | tf_op jit(solution)/shard_map/reduce_scatter | solution.py:59
  332.8 2.6 multiply_add_fusion
  335.5 147.8 %reduce-scatter.9.cloned.1.call-done = f32[256,1024]{0,1:T(8,128)} async-done(((f32[2048,1024]{0,1:T(8,128)}), f32[256,1024]{0,1:T(8,128)}) %reduce-scatter.9.cloned.1.call-update) | async-done | bytes 1048592 | tf_op jit(solution)/shard_map/reduce_scatter | solution.py:54
  483.3 2.3 multiply_add_fusion.1
  485.6 2.5 copy.14
  488.2 28.4 %reduce-scatter.7.cloned.1.call-done = bf16[128,2048]{1,0:T(8,128)(2,1)} async-done(((bf16[512,2048]{1,0:T(8,128)(2,1)}), bf16[128,2048]{1,0:T(8,128)(2,1)}) %reduce-scatter.7.cloned.1.call-update) | async-done | bytes 524304 | tf_op jit(solution)/shard_map/reduce_scatter | solution.py:47
  516.6 34.3 %reduce-scatter.5.cloned.1.call-done = bf16[128,2048]{1,0:T(8,128)(2,1)} async-done(((bf16[512,2048]{1,0:T(8,128)(2,1)}), bf16[128,2048]{1,0:T(8,128)(2,1)}) %reduce-scatter.5.cloned.1.call-update) | async-done | bytes 524304 | tf_op jit(solution)/shard_map/reduce_scatter | solution.py:37
  (21 shorter events, 0.3 us)
Async XLA Ops:
  7.2 2.3 copy-start
  7.2 78.5 %all-gather.8.cloned.1.call-start = ((), (), s32[]{:S(2)}) async-start(), calls=%async_computation.6 | async-start | bytes 4718592 | tf_op jit(solution)/shard_map/all_gather | solution.py:29
  7.9 151.2 %all-gather.6.cloned.1.call-start = ((), (), s32[]{:S(2)}) async-start(), calls=%async_computation.5 | async-start | bytes 4718592 | tf_op jit(solution)/shard_map/all_gather | solution.py:28
  8.7 173.2 %all-gather.4.cloned.1.call-start = ((), (), s32[]{:S(2)}) async-start(), calls=%async_computation.4 | async-start | bytes 2621440 | tf_op jit(solution)/shard_map/all_gather | solution.py:22
  9.4 323.4 %reduce-scatter.11.cloned.1.call-start = ((), (), s32[]{:S(2)}) async-start(), calls=%async_computation.10 | async-start | bytes 9437184 | tf_op jit(solution)/shard_map/reduce_scatter | solution.py:59
  16.3 69.3 %copy-start.3 = (bf16[512,1024]{1,0:T(8,128)(2,1)S(1)}, bf16[512,1024]{1,0:T(8,128)(2,1)}, u32[]{:S(2)}) copy-start(bf16[512,1024]{1,0:T(8,128)(2,1)} %param.10) | copy-start | bytes 3145732
  16.3 467.0 %reduce-scatter.9.cloned.1.call-start = ((), (), s32[]{:S(2)}) async-start(), calls=%async_computation.9 | async-start | bytes 9437184 | tf_op jit(solution)/shard_map/reduce_scatter | solution.py:54
  85.7 5.7 %copy-start.2 = (bf16[512,2048]{1,0:T(8,128)(2,1)S(1)}, bf16[512,2048]{1,0:T(8,128)(2,1)}, u32[]{:S(2)}) copy-start(bf16[512,2048]{1,0:T(8,128)(2,1)} %param.9) | copy-start | bytes 6291460
  90.4 1.0 copy-start.5
  97.0 62.2 %copy-start.6 = (bf16[512,1024]{1,0:T(8,128)(2,1)S(1)}, bf16[512,1024]{1,0:T(8,128)(2,1)}, u32[]{:S(2)}) copy-start(bf16[512,1024]{1,0:T(8,128)(2,1)} %copy-done.5) | copy-start | bytes 3145732
  97.0 419.6 %reduce-scatter.7.cloned.1.call-start = ((), (), s32[]{:S(2)}) async-start(), calls=%async_computation.8 | async-start | bytes 2621440 | tf_op jit(solution)/shard_map/reduce_scatter | solution.py:47
  165.1 385.8 %reduce-scatter.5.cloned.1.call-start = ((), (), s32[]{:S(2)}) async-start(), calls=%async_computation.7 | async-start | bytes 2621440 | tf_op jit(solution)/shard_map/reduce_scatter | solution.py:37
  181.8 6.3 %copy-start.1 = (bf16[1024,2048]{1,0:T(8,128)(2,1)S(1)}, bf16[1024,2048]{1,0:T(8,128)(2,1)}, u32[]{:S(2)}) copy-start(bf16[1024,2048]{1,0:T(8,128)(2,1)} %all-gather.8.cloned.1.call-done) | copy-start | bytes 12582916
  187.1 1.0 copy-start.4
Sparse Core Ops, SparseCore 0:
  10.1 75.5 all-gather.7
  87.8 71.3 all-gather.5
  160.7 21.0 all-gather.3
  185.3 147.4 reduce-scatter.10
  336.3 146.9 reduce-scatter.8
  486.3 30.2 reduce-scatter.6
  519.7 31.1 reduce-scatter.4
where the time goes:
time: 558 us
  waiting for transfers between devices  500 us (90%)
  matrix products  32.1 us (6%)
  between operations  14.2 us (3%)
  local copies, waits for them, and re-layouts  6.36 us (1%)
    reduce_scatter x1, waiting for transfers between devices, shards(): lax.psum_scatter(contract_first(columns, pre_grad), 'fs', scatter_dimensi...  148 us
    reduce_scatter x1, waiting for transfers between devices, shards(): lax.psum_scatter(contract_first(columns, cotangent), 'fs', scatter_dimens...  139 us
    all_gather x1, waiting for transfers between devices, shards(): lax.all_gather(down_weight, 'fs', axis=0, tiled=True)  69.3 us
    all_gather x1, waiting for transfers between devices, shards(): lax.all_gather(up_weight, 'fs', axis=0, tiled=True)  62.1 us
    reduce_scatter x1, waiting for transfers between devices, shards(): lax.psum_scatter(jnp.dot(rows_here, down_front, preferred_element_type=jn...  34.3 us
    reduce_scatter x1, waiting for transfers between devices, shards(): lax.psum_scatter(contract_last(rows_here, up_back).astype(jnp.bfloat16),...  28.4 us
    all_gather x1, waiting for transfers between devices, shards(): gathered = lax.all_gather(later_input, 'tp', axis=0, tiled=True)  16.5 us
    dot_general x2, matrix products, contract_first(): lax.dot_general(left_rows, right_rows, (((0,), (0,)), ((), ())), preferre...  12.5 us
  transfers between devices with their start and end apart: 7, of which 7 were waited for; matrix products, arithmetic and copies ran while one was open for 7% of the time, Pallas kernels for 0%

commit v1 on v0

--- a/solution.py
+++ b/solution.py
@@ -2,6 +2,19 @@
 import jax.numpy as jnp
 from jax import lax
 from jax.sharding import PartitionSpec as P
+
+
+def gather_around(x, axis, dim):
+    ways = lax.axis_size(axis)
+    up = [(d, (d + 1) % ways) for d in range(ways)]
+    down = [(d, (d - 1) % ways) for d in range(ways)]
+    earlier, later = ([x], [x])
+    for _ in range(ways // 2):
+        earlier.append(lax.ppermute(earlier[-1], axis, up))
+    for _ in range((ways - 1) // 2):
+        later.append(lax.ppermute(later[-1], axis, down))
+    line = jnp.concatenate([*earlier[::-1], *later[1:]], axis=dim)
+    return jnp.roll(line, (lax.axis_index(axis) - ways // 2) * x.shape[dim], axis=dim)
 
 
 def contract_last(left_rows, right_rows):
@@ -25,7 +38,7 @@
     lifted = jnp.maximum(earlier_hidden.astype(jnp.float32), 0.0)
     activation = (lifted * lifted).astype(jnp.bfloat16)
     up_front, down_front = (
-        lax.all_gather(up_weight, "fs", axis=0, tiled=True),
+        gather_around(up_weight, "fs", 0),
         lax.all_gather(down_weight, "fs", axis=0, tiled=True),
     )
     later_hidden = jnp.dot(gathered, up_front, preferred_element_type=jnp.float32).astype(

time: 558 us -> 520 us (0.932)
  waiting for transfers between devices: 500 us -> 427 us
  starting transfers between devices: 0.46 us -> 21.4 us
  local copies, waits for them, and re-layouts: 6.36 us -> 23.1 us
    ppermute x0 -> x7, waiting for transfers between devices: none -> 82.5 us  [the longest x4 74.9 us: gather_around(): earlier.append(lax.ppermute(earlier[-1], axis, up))]
    reduce_scatter x1, waiting for transfers between devices: 139 us -> 63.1 us  [shards(): lax.psum_scatter(contract_first(columns, cotangent), 'fs', scatter_dimens...]
    all_gather x1 -> x0, waiting for transfers between devices: 62.1 us -> none  [shards(): lax.all_gather(up_weight, 'fs', axis=0, tiled=True)]
    ppermute x0 -> x7, starting transfers between devices: none -> 21 us  [the longest x3 17.9 us: gather_around(): later.append(lax.ppermute(later[-1], axis, down))]
    unnamed x16 -> x39, local copies, waits for them, and re-layouts: 6.36 us -> 23 us
    all_gather x1, waiting for transfers between devices: 16.5 us -> 0.02 us  [shards(): gathered = lax.all_gather(later_input, 'tp', axis=0, tiled=True)]
  transfers between devices with their start and end apart: 7 -> 13, of which waited for: 7 -> 11; matrix products, arithmetic and copies ran while one was open for 7% -> 10% of each run, Pallas kernels for 0% -> 0%
where the time goes in v1:
time: 520 us
  waiting for transfers between devices  427 us (82%)
  matrix products  28.7 us (6%)
  local copies, waits for them, and re-layouts  23.1 us (4%)
  starting transfers between devices  21.4 us (4%)
  between operations  14.3 us (3%)
    reduce_scatter x1, waiting for transfers between devices, shards(): lax.psum_scatter(contract_first(columns, pre_grad), 'fs', scatter_dimensi...  148 us
    ppermute x4, waiting for transfers between devices, gather_around(): earlier.append(lax.ppermute(earlier[-1], axis, up))  74.9 us
    all_gather x1, waiting for transfers between devices, shards(): lax.all_gather(down_weight, 'fs', axis=0, tiled=True)  69.8 us
    reduce_scatter x1, waiting for transfers between devices, shards(): lax.psum_scatter(contract_first(columns, cotangent), 'fs', scatter_dimens...  63.1 us
    reduce_scatter x1, waiting for transfers between devices, shards(): lax.psum_scatter(jnp.dot(rows_here, down_front, preferred_element_type=jn...  34.2 us
    reduce_scatter x1, waiting for transfers between devices, shards(): lax.psum_scatter(contract_last(rows_here, up_back).astype(jnp.bfloat16),...  28.4 us
    unnamed x39, local copies, waits for them, and re-layouts  23 us
    ppermute x3, starting transfers between devices, gather_around(): later.append(lax.ppermute(later[-1], axis, down))  17.9 us
  transfers between devices with their start and end apart: 13, of which 11 were waited for; matrix products, arithmetic and copies ran while one was open for 10% of the time, Pallas kernels for 0%

profile of v1, /device:TPU:0, one launch (start us, length us, event | category | flops | bytes accessed | tf_op | source)
XLA Modules:
  0.0 519.6 jit_solution(17361724582019339988)
XLA Ops:
  10.2 5.6 %fusion.13 = f32[1024,2048]{1,0:T(8,128)} fusion(bf16[512,2048]{1,0:T(8,128)(2,1)S(1)} %copy-done, bf16[512,1024]{0,1:T(8,128)(2,1)S(1)} %copy.14), kind=kOutput, calls=%fused_computation.13 | convolution fusion | flops 2149580800 | bytes 11534336 | tf_op jit(solution)/shard_map/dot_general | solution.py:27
  15.9 69.8 %all-gather.5.cloned.1.call-done = bf16[1024,2048]{1,0:T(8,128)(2,1)} async-done(((bf16[128,2048]{1,0:T(8,128)(2,1)}), bf16[1024,2048]{1,0:T(8,128)(2,1)}) %all-gather.5.cloned.1.call-update) | async-done | bytes 4194320 | tf_op jit(solution)/shard_map/all_gather | solution.py:42
  85.7 4.7 multiply_convert_fusion.1
  91.4 5.6 %convolution_bitcast_fusion = f32[2048,1024]{0,1:T(8,128)} fusion(bf16[512,1024]{0,1:T(8,128)(2,1)S(1)} %multiply_convert_fusion.1, bf16[512,2048]{1,0:T(8,128)(2,1)S(1)} %copy-done.7), kind=kOutput, calls=%fused_computation | convolution fusion | flops 2147483648 | bytes 11534336 | tf_op jit(solution)/shard_map/dot_general | solution.py:27
  97.6 14.6 %collective-permute-done = bf16[256,1024]{1,0:T(8,128)(2,1)S(1)} collective-permute-done((bf16[256,1024]{1,0:T(8,128)(2,1)S(1)}, bf16[256,1024]{1,0:T(8,128)(2,1)S(1)}, u32[]{:S(2)}, u32[]{:S(2)}) %collective-permute-start) | collective-permute-done | bytes 524320 | tf_op jit(solution)/shard_map/ppermute | solution.py:13
  112.2 4.7 collective-permute-start.4
  117.0 27.1 %collective-permute-done.1 = bf16[256,1024]{1,0:T(8,128)(2,1)S(1)} collective-permute-done((bf16[256,1024]{1,0:T(8,128)(2,1)S(1)}, bf16[256,1024]{1,0:T(8,128)(2,1)S(1)}, u32[]{:S(2)}, u32[]{:S(2)}) %collective-permute-start.1) | collective-permute-done | bytes 524320 | tf_op jit(solution)/shard_map/ppermute | solution.py:13
  144.1 2.5 collective-permute-start.2
  146.6 8.0 %collective-permute-start.5 = (bf16[256,1024]{1,0:T(8,128)(2,1)}, bf16[256,1024]{1,0:T(8,128)(2,1)}, u32[]{:S(2)}, u32[]{:S(2)}) collective-permute-start(bf16[256,1024]{1,0:T(8,128)(2,1)} %collective-permute-done.4), channel_id=1, source_target_pairs={{0,28},{4,0},{8,4},{12,8},{16,12},{20,16},{24,20},{28,24},{1,29},{... | collective-permute-start | bytes 1572872 | tf_op jit(solution)/shard_map/ppermute | solution.py:15
  154.6 16.7 %collective-permute-done.2 = bf16[256,1024]{1,0:T(8,128)(2,1)} collective-permute-done((bf16[256,1024]{1,0:T(8,128)(2,1)S(1)}, bf16[256,1024]{1,0:T(8,128)(2,1)}, u32[]{:S(2)}, u32[]{:S(2)}) %collective-permute-start.2) | collective-permute-done | bytes 524320 | tf_op jit(solution)/shard_map/ppermute | solution.py:13
  171.3 6.5 %collective-permute-done.5 = bf16[256,1024]{1,0:T(8,128)(2,1)} collective-permute-done((bf16[256,1024]{1,0:T(8,128)(2,1)}, bf16[256,1024]{1,0:T(8,128)(2,1)}, u32[]{:S(2)}, u32[]{:S(2)}) %collective-permute-start.5) | collective-permute-done | bytes 524320 | tf_op jit(solution)/shard_map/ppermute | solution.py:15
  177.8 5.2 collective-permute-start.6
  183.0 16.4 %collective-permute-done.3 = bf16[256,1024]{1,0:T(8,128)(2,1)} collective-permute-done((bf16[256,1024]{1,0:T(8,128)(2,1)}, bf16[256,1024]{1,0:T(8,128)(2,1)}, u32[]{:S(2)}, u32[]{:S(2)}) %collective-permute-start.3) | collective-permute-done | bytes 524320 | tf_op jit(solution)/shard_map/ppermute | solution.py:13
  210.6 3.2 copy-done.5
  213.9 3.7 fusion.4
  217.8 5.4 %fusion.10 = bf16[512,1024]{0,1:T(8,128)(2,1)S(1)} fusion(bf16[512,2048]{1,0:T(8,128)(2,1)} %all-gather.3.cloned.1.call-done, bf16[4096,1024]{1,0:T(8,128)(2,1)} %copy-done.5, s32[]{:T(128)S(6)} %select_n.14), kind=kOutput, calls=%fused_computation.12 | convolution fusion | flops 2148007936 | bytes 7340036 | tf_op jit(solution)/shard_map/dot_general | solution.py:44
  224.2 3.7 convolution_convert_fusion
  231.8 63.1 %reduce-scatter.11.cloned.1.call-done = f32[128,2048]{1,0:T(8,128)} async-done(((f32[1024,2048]{1,0:T(8,128)}), f32[128,2048]{1,0:T(8,128)}) %reduce-scatter.11.cloned.1.call-update) | async-done | bytes 1048592 | tf_op jit(solution)/shard_map/reduce_scatter | solution.py:72
  294.9 2.6 multiply_add_fusion
  297.5 147.8 %reduce-scatter.9.cloned.1.call-done = f32[256,1024]{0,1:T(8,128)} async-done(((f32[2048,1024]{0,1:T(8,128)}), f32[256,1024]{0,1:T(8,128)}) %reduce-scatter.9.cloned.1.call-update) | async-done | bytes 1048592 | tf_op jit(solution)/shard_map/reduce_scatter | solution.py:67
  445.3 2.3 multiply_add_fusion.1
  447.7 2.5 copy.17
  450.2 28.4 %reduce-scatter.7.cloned.1.call-done = bf16[128,2048]{1,0:T(8,128)(2,1)} async-done(((bf16[512,2048]{1,0:T(8,128)(2,1)}), bf16[128,2048]{1,0:T(8,128)(2,1)}) %reduce-scatter.7.cloned.1.call-update) | async-done | bytes 524304 | tf_op jit(solution)/shard_map/reduce_scatter | solution.py:60
  478.6 34.2 %reduce-scatter.5.cloned.1.call-done = bf16[128,2048]{1,0:T(8,128)(2,1)} async-done(((bf16[512,2048]{1,0:T(8,128)(2,1)}), bf16[128,2048]{1,0:T(8,128)(2,1)}) %reduce-scatter.5.cloned.1.call-update) | async-done | bytes 524304 | tf_op jit(solution)/shard_map/reduce_scatter | solution.py:50
  (56 shorter events, 20.9 us)
Async XLA Ops:
  7.2 3.1 copy-start
  7.2 78.5 %all-gather.5.cloned.1.call-start = ((), (), s32[]{:S(2)}) async-start(), calls=%async_computation.5 | async-start | bytes 4718592 | tf_op jit(solution)/shard_map/all_gather | solution.py:42
  7.9 209.9 %all-gather.3.cloned.1.call-start = ((), (), s32[]{:S(2)}) async-start(), calls=%async_computation.4 | async-start | bytes 2621440 | tf_op jit(solution)/shard_map/all_gather | solution.py:35
  8.7 286.2 %reduce-scatter.11.cloned.1.call-start = ((), (), s32[]{:S(2)}) async-start(), calls=%async_computation.9 | async-start | bytes 9437184 | tf_op jit(solution)/shard_map/reduce_scatter | solution.py:72
  15.8 429.5 %reduce-scatter.9.cloned.1.call-start = ((), (), s32[]{:S(2)}) async-start(), calls=%async_computation.8 | async-start | bytes 9437184 | tf_op jit(solution)/shard_map/reduce_scatter | solution.py:67
  85.7 5.7 %copy-start.7 = (bf16[512,2048]{1,0:T(8,128)(2,1)S(1)}, bf16[512,2048]{1,0:T(8,128)(2,1)}, u32[]{:S(2)}) copy-start(bf16[512,2048]{1,0:T(8,128)(2,1)} %param.9) | copy-start | bytes 6291460
  90.4 1.0 copy-start.8
  91.4 5.7 %copy-start.1 = (bf16[256,1024]{1,0:T(8,128)(2,1)S(1)}, bf16[256,1024]{1,0:T(8,128)(2,1)}, u32[]{:S(2)}) copy-start(bf16[256,1024]{1,0:T(8,128)(2,1)} %param.12) | copy-start | bytes 1572868
  97.0 381.6 %reduce-scatter.7.cloned.1.call-start = ((), (), s32[]{:S(2)}) async-start(), calls=%async_computation.7 | async-start | bytes 2621440 | tf_op jit(solution)/shard_map/reduce_scatter | solution.py:60
  97.0 15.2 %collective-permute-start = (bf16[256,1024]{1,0:T(8,128)(2,1)S(1)}, bf16[256,1024]{1,0:T(8,128)(2,1)S(1)}, u32[]{:S(2)}, u32[]{:S(2)}) collective-permute-start(bf16[256,1024]{1,0:T(8,128)(2,1)S(1)} %copy-done.1), channel_id=1, source_target_pairs={{0,4},{4,8},{8,12},{12,16},{16,20},{20,24},{24,28},{28,0},{1,5},{5... | collective-permute-start | bytes 1572872 | tf_op jit(solution)/shard_map/ppermute | solution.py:13
  112.2 31.9 %collective-permute-start.1 = (bf16[256,1024]{1,0:T(8,128)(2,1)S(1)}, bf16[256,1024]{1,0:T(8,128)(2,1)S(1)}, u32[]{:S(2)}, u32[]{:S(2)}) collective-permute-start(bf16[256,1024]{1,0:T(8,128)(2,1)S(1)} %collective-permute-done), channel_id=1, source_target_pairs={{0,4},{4,8},{8,12},{12,16},{16,20},{20,24},{24,28},{28,0},{1,5},{5... | collective-permute-start | bytes 1572872 | tf_op jit(solution)/shard_map/ppermute | solution.py:13
  112.2 34.3 %collective-permute-start.4 = (bf16[256,1024]{1,0:T(8,128)(2,1)S(1)}, bf16[256,1024]{1,0:T(8,128)(2,1)}, u32[]{:S(2)}, u32[]{:S(2)}) collective-permute-start(bf16[256,1024]{1,0:T(8,128)(2,1)S(1)} %copy-done.1), channel_id=1, source_target_pairs={{0,28},{4,0},{8,4},{12,8},{16,12},{20,16},{24,20},{28,24},{1,29},{... | collective-permute-start | bytes 1572872 | tf_op jit(solution)/shard_map/ppermute | solution.py:15
  144.1 2.5 copy-start.2
  144.1 27.2 %collective-permute-start.2 = (bf16[256,1024]{1,0:T(8,128)(2,1)S(1)}, bf16[256,1024]{1,0:T(8,128)(2,1)}, u32[]{:S(2)}, u32[]{:S(2)}) collective-permute-start(bf16[256,1024]{1,0:T(8,128)(2,1)S(1)} %collective-permute-done.1), channel_id=1, source_target_pairs={{0,4},{4,8},{8,12},{12,16},{16,20},{20,24},{24,28},{28,0},{1,5},{5... | collective-permute-start | bytes 1572872 | tf_op jit(solution)/shard_map/ppermute | solution.py:13
  146.6 31.2 %collective-permute-start.5 = (bf16[256,1024]{1,0:T(8,128)(2,1)}, bf16[256,1024]{1,0:T(8,128)(2,1)}, u32[]{:S(2)}, u32[]{:S(2)}) collective-permute-start(bf16[256,1024]{1,0:T(8,128)(2,1)} %collective-permute-done.4), channel_id=1, source_target_pairs={{0,28},{4,0},{8,4},{12,8},{16,12},{20,16},{24,20},{28,24},{1,29},{... | collective-permute-start | bytes 1572872 | tf_op jit(solution)/shard_map/ppermute | solution.py:15
  171.3 28.1 %collective-permute-start.3 = (bf16[256,1024]{1,0:T(8,128)(2,1)}, bf16[256,1024]{1,0:T(8,128)(2,1)}, u32[]{:S(2)}, u32[]{:S(2)}) collective-permute-start(bf16[256,1024]{1,0:T(8,128)(2,1)} %collective-permute-done.2), channel_id=1, source_target_pairs={{0,4},{4,8},{8,12},{12,16},{16,20},{20,24},{24,28},{28,0},{1,5},{5... | collective-permute-start | bytes 1572872 | tf_op jit(solution)/shard_map/ppermute | solution.py:13
  171.3 37.0 %copy-start.3 = (bf16[256,1024]{1,0:T(8,128)(2,1)S(1)}, bf16[256,1024]{1,0:T(8,128)(2,1)}, u32[]{:S(2)}) copy-start(bf16[256,1024]{1,0:T(8,128)(2,1)} %copy-done.2) | copy-start | bytes 1572868
  171.3 42.6 %copy-start.9 = (bf16[512,1024]{0,1:T(8,128)(2,1)S(1)}, bf16[512,1024]{0,1:T(8,128)(2,1)}, u32[]{:S(2)}) copy-start(bf16[512,1024]{0,1:T(8,128)(2,1)} %copy-done.8) | copy-start | bytes 3145732
  177.8 28.2 %collective-permute-start.6 = (bf16[256,1024]{1,0:T(8,128)(2,1)}, bf16[256,1024]{1,0:T(8,128)(2,1)S(1)}, u32[]{:S(2)}, u32[]{:S(2)}) collective-permute-start(bf16[256,1024]{1,0:T(8,128)(2,1)} %collective-permute-done.5), channel_id=1, source_target_pairs={{0,28},{4,0},{8,4},{12,8},{16,12},{20,16},{24,20},{28,24},{1,29},{... | collective-permute-start | bytes 1572872 | tf_op jit(solution)/shard_map/ppermute | solution.py:15
  210.6 3.3 copy-start.5
  217.6 295.2 %reduce-scatter.5.cloned.1.call-start = ((), (), s32[]{:S(2)}) async-start(), calls=%async_computation.6 | async-start | bytes 2621440 | tf_op jit(solution)/shard_map/reduce_scatter | solution.py:50
  217.8 6.4 %copy-start.6 = (bf16[1024,2048]{1,0:T(8,128)(2,1)S(1)}, bf16[1024,2048]{1,0:T(8,128)(2,1)}, u32[]{:S(2)}) copy-start(bf16[1024,2048]{1,0:T(8,128)(2,1)} %all-gather.5.cloned.1.call-done) | copy-start | bytes 12582916
  223.2 1.0 copy-start.4
Sparse Core Ops, SparseCore 0:
  10.1 75.5 all-gather.4
  87.2 21.0 all-gather.2
  112.0 182.8 reduce-scatter.10
  298.4 146.9 reduce-scatter.8
  448.3 30.2 reduce-scatter.6
  481.6 31.1 reduce-scatter.4
